TPU v7x, 512 devices: a whole 4x8x8 slice. The times are simulated.
512 devices in a mesh: sp: 32 (over z, x), tp: 16 (over y, core).
Axes of the slice: x: 4, y: 8, z: 8, core: 2. Of those that a mesh axis runs over, the one named last changes fastest.
Arguments:
- queries: bfloat16 [8192, 1024], P('sp', 'tp'), may hold values from -6 to 6
- keys: bfloat16 [8192, 256], P('sp'), may hold values from -6 to 6
- values: bfloat16 [8192, 256], P('sp'), may hold values from -6 to 6
- sink: float32 [16], P('tp'), may hold values from 3 to 6
- w_out: bfloat16 [1024, 2048], P('tp'), may hold values from -0.1875 to 0.1875
- stream: bfloat16 [8192, 2048], P(('sp', 'tp')), may hold values from -6 to 6
- gain: bfloat16 [2048], replicated, may hold values from 0.099609375 to 1.8984375
- routes: int32 [8192, 4], P('sp'), may hold values from 0 to 63, all different within a row; in each aligned block of 16 rows (0 to 15, 16 to 31, ...) at most 2 rows name the same one
- route_weights: float32 [8192, 4], P('sp'), may hold values from 0.2 to 1
- w_gate: bfloat16 [64, 1024, 2048], P('sp', 'tp'), may hold values from -0.125 to 0.125
- w_up: bfloat16 [64, 1024, 2048], P('sp', 'tp'), may hold values from -0.125 to 0.125
- w_down: bfloat16 [64, 1024, 2048], P('sp', None, 'tp'), may hold values from -0.1875 to 0.1875
- shared_gate: bfloat16 [1024, 2048], P('tp'), may hold values from -0.125 to 0.125
- shared_up: bfloat16 [1024, 2048], P('tp'), may hold values from -0.125 to 0.125
- shared_down: bfloat16 [1024, 2048], P(None, 'tp'), may hold values from -0.1875 to 0.1875
Outputs:
- layer_out: bfloat16 [8192, 2048], P('sp', 'tp')
Inputs may be any that keep to these rules, and one draw needn't show every extreme that they name: `routes`: in each aligned block of 16 rows no expert is named in more than 2 rows, and some blocks reach 2; a row names 4 different experts.
All inputs are finite; a program needn't handle non-finite values.
Results may differ from a plain program's by a relative error of at most 0.014.
Values may be sent and summed in bfloat16 or wider, within the bound.
A program may use at most 64 MiB of HBM per device.

v0:
```python
import jax
import jax.numpy as jnp
from jax import lax
from jax.sharding import PartitionSpec as P

D = 2048
HEADS = 16
KV_HEADS = 4
HD = 64
WINDOW = 128
EXPERTS = 64
TOPK = 4
NORM_EPS = 1e-05


def with_halo(array, sides, width):
    for axis, dim in sides:
        devices, length = (lax.axis_size(axis), array.shape[dim])
        up = [(i, (i + 1) % devices) for i in range(devices - 1)]
        down = [(j, i) for i, j in up]
        last = lax.slice_in_dim(array, length - width, length, axis=dim)
        leading = lax.slice_in_dim(array, 0, width, axis=dim)
        before = lax.ppermute(last, axis, up)
        after = lax.ppermute(leading, axis, down)
        array = jnp.concatenate([before, array, after], axis=dim)
    return array


def laid_out(tiles, dim):
    tiles = jnp.moveaxis(tiles, 0, dim)
    dims = tiles.shape
    return tiles.reshape(*dims[:dim], dims[dim] * dims[dim + 1], *dims[dim + 2 :])


def from_everyone(array, axis):
    copies = jnp.broadcast_to(array, (lax.axis_size(axis), *array.shape))
    return lax.all_to_all(copies, axis, split_axis=0, concat_axis=0, tiled=True)


def gathered_copies(array, axis, dim):
    return laid_out(from_everyone(array, axis), dim)


def taken_together(array, axis):
    return from_everyone(array, axis).sum(axis=0)


def gather_turned(arrays, axis, dims):
    turned = [jnp.moveaxis(a, dim, 0) for a, dim in zip(arrays, dims)]
    widths = [t[0].size for t in turned]
    both = jnp.concatenate([t.reshape(-1, w) for t, w in zip(turned, widths)], axis=1)
    result = lax.all_gather(both, axis, axis=0, tiled=True)
    tiles = jnp.split(result, [sum(widths[:k]) for k in range(1, len(widths))], axis=1)
    return tuple(
        (
            jnp.moveaxis(b.reshape(-1, *t.shape[1:]), 0, dim)
            for b, t, dim in zip(tiles, turned, dims)
        )
    )


def slot_ids(block_routes, capacity):
    flat_routes = block_routes.reshape(-1)
    hit_table = (flat_routes[:, None] == jnp.arange(EXPERTS)[None, :]).astype(jnp.int32)
    earlier = jnp.cumsum(hit_table, axis=0) - hit_table
    slot_rank = jnp.sum(earlier * hit_table, axis=1)
    return flat_routes * capacity + slot_rank


def local(
    queries,
    keys,
    values,
    sink,
    w_out,
    stream,
    gain,
    routes,
    route_weights,
    w_gate,
    w_up,
    w_down,
    shared_gate,
    shared_up,
    shared_down,
):
    tok_dev = queries.shape[0]
    n_tp = lax.axis_size("tp")
    n_sp = lax.axis_size("sp")
    tp_idx = lax.axis_index("tp")
    sp_idx = lax.axis_index("sp")
    heads_dev = HEADS // n_tp
    group = HEADS // KV_HEADS
    kv_head = tp_idx * heads_dev // group
    key_own = lax.dynamic_slice_in_dim(keys, kv_head * HD, HD, 1)
    value_own = lax.dynamic_slice_in_dim(values, kv_head * HD, HD, 1)
    paired = jnp.concatenate([key_own, value_own], axis=1)
    padded = with_halo(paired, (("sp", 0),), WINDOW)
    blocks = tok_dev // WINDOW
    framed = padded.reshape(blocks + 2, WINDOW, 2 * HD)
    banded = jnp.concatenate([framed[:-2], framed[1:-1], framed[2:]], axis=1)
    key_band = banded[:, :, :HD]
    value_band = banded[:, :, HD:]
    query_blocks = queries.reshape(blocks, WINDOW, heads_dev, HD)
    scores = jnp.einsum(
        "nqhd,njd->nhqj", query_blocks, key_band, preferred_element_type=jnp.float32
    ) * HD ** (-0.5)
    offset = sp_idx * tok_dev
    seq_total = tok_dev * n_sp
    query_pos = (
        offset + jnp.arange(blocks)[:, None, None] * WINDOW + jnp.arange(WINDOW)[None, :, None]
    )
    key_pos = (
        offset
        - WINDOW
        + jnp.arange(blocks)[:, None, None] * WINDOW
        + jnp.arange(3 * WINDOW)[None, None, :]
    )
    allowed = (jnp.abs(query_pos - key_pos) <= WINDOW) & (key_pos >= 0) & (key_pos < seq_total)
    scores = jnp.where(allowed[:, None], scores, -jnp.inf)
    sink_level = sink.reshape(1, heads_dev, 1, 1)
    row_peak = jnp.maximum(scores.max(-1, keepdims=True), sink_level)
    probabilities = jnp.exp(scores - row_peak)
    denominator = probabilities.sum(-1, keepdims=True) + jnp.exp(sink_level - row_peak)
    weights = (probabilities / denominator).astype(jnp.bfloat16)
    attended = jnp.einsum("nhqj,njd->nqhd", weights, value_band, preferred_element_type=jnp.float32)
    attended = attended.astype(jnp.bfloat16).reshape(tok_dev, heads_dev * HD)
    rows_dev = tok_dev // n_tp
    d_dev = w_down.shape[2]
    all_heads = gathered_copies(attended, "tp", 1)
    w_cols, stream_cols = (
        lax.all_to_all(w_out, "tp", split_axis=1, concat_axis=0, tiled=True),
        lax.all_to_all(stream, "tp", split_axis=1, concat_axis=0, tiled=True),
    )
    projected = jnp.dot(all_heads, w_cols, preferred_element_type=jnp.float32)
    mixed_cols = (stream_cols.astype(jnp.float32) + projected).astype(jnp.bfloat16)
    residual = mixed_cols.astype(jnp.float32)
    square_sum = taken_together(jnp.sum(residual * residual, axis=-1), "tp")
    scale_rows = lax.rsqrt(square_sum[:, None] / D + NORM_EPS)
    gain_cols = lax.dynamic_slice_in_dim(gain, tp_idx * d_dev, d_dev, 0).astype(jnp.float32)
    normed_cols = (residual * scale_rows * gain_cols[None, :]).astype(jnp.bfloat16)
    normed = gathered_copies(normed_cols, "tp", 1)
    exp_dev = w_gate.shape[0]
    capacity = max(1, 2 * tok_dev * TOPK // (n_tp * EXPERTS))
    slot_count = EXPERTS * capacity
    blocked_routes = routes.reshape(n_tp, rows_dev, TOPK)
    destination = jax.vmap(lambda block_routes: slot_ids(block_routes, capacity))(blocked_routes)
    slot_select = destination[:, None, :] == jnp.arange(slot_count)[None, :, None]
    slot_select = slot_select.reshape(n_tp, slot_count, rows_dev, TOPK).astype(jnp.float32)
    dispatch_table = jnp.sum(slot_select, axis=-1).astype(jnp.bfloat16)
    combine_table = jnp.sum(slot_select * route_weights.reshape(n_tp, 1, rows_dev, TOPK), axis=-1)
    normed_blocks = normed.reshape(n_tp, rows_dev, D)
    own_table = lax.dynamic_index_in_dim(dispatch_table, tp_idx, 0, keepdims=False)
    own_rows = lax.dynamic_index_in_dim(normed_blocks, tp_idx, 0, keepdims=False)
    outgoing = jnp.dot(own_table, own_rows, preferred_element_type=jnp.float32).astype(jnp.bfloat16)
    arrived = lax.all_to_all(outgoing, "sp", split_axis=0, concat_axis=0, tiled=True)
    arrived = arrived.reshape(1, n_sp, exp_dev, capacity, D)
    piece_rows = lax.all_gather(arrived, "tp", axis=0, tiled=True)
    gate_act = jnp.einsum(
        "tsecd,efd->tsecf", piece_rows, w_gate, preferred_element_type=jnp.float32
    )
    up_act = jnp.einsum("tsecd,efd->tsecf", piece_rows, w_up, preferred_element_type=jnp.float32)
    hidden = (jax.nn.silu(gate_act) * up_act).astype(jnp.bfloat16)
    shared_gate_act = jnp.einsum(
        "td,fd->tf", normed, shared_gate, preferred_element_type=jnp.float32
    )
    shared_up_act = jnp.einsum("td,fd->tf", normed, shared_up, preferred_element_type=jnp.float32)
    shared_hidden = (jax.nn.silu(shared_gate_act) * shared_up_act).astype(jnp.bfloat16)
    shared_hidden = shared_hidden.reshape(1, 1, 1, tok_dev, shared_hidden.shape[1])
    expert_piece, shared_piece = gather_turned((hidden, shared_hidden), "tp", (4, 4))
    piece_width = expert_piece.shape[4]
    routed_total = jnp.einsum(
        "tsecf,efd->tsecd", expert_piece, w_down, preferred_element_type=jnp.float32
    )
    shared_total = jnp.dot(
        shared_piece.reshape(tok_dev, piece_width), shared_down, preferred_element_type=jnp.float32
    )
    returned = lax.all_to_all(
        routed_total.astype(jnp.bfloat16), "sp", split_axis=1, concat_axis=1, tiled=True
    )
    returned = returned.reshape(n_tp, slot_count, d_dev).astype(jnp.float32)
    routed = jnp.einsum("tmr,tmd->trd", combine_table, returned)
    routed = routed.reshape(tok_dev, d_dev)
    return (residual + routed + shared_total).astype(jnp.bfloat16)


def solution(mesh):
    placed = (
        P("sp", "tp"),
        P("sp", None),
        P("sp", None),
        P("tp"),
        P("tp", None),
        P(("sp", "tp"), None),
        P(),
        P("sp", None),
        P("sp", None),
        P("sp", "tp", None),
        P("sp", "tp", None),
        P("sp", None, "tp"),
        P("tp", None),
        P("tp", None),
        P(None, "tp"),
    )
    return jax.shard_map(
        local, mesh=mesh, in_specs=placed, out_specs=P("sp", "tp"), check_vma=False
    )
```

profile of v0, /device:TPU:8, one launch (start us, length us, event | category | flops | bytes accessed | tf_op | source)
XLA Modules:
  0.0 313.8 jit_solution(5770819059560762188)
XLA Ops:
  6.5 1.5 copy_bitcast_fusion.1
  8.1 9.1 %all-to-all-start = ((bf16[16,16,128]{2,0,1:T(8,128)(2,1)}), bf16[16,16,128]{2,0,1:T(8,128)(2,1)S(1)}, u32[]{:S(2)}, u32[]{:S(2)}) async-start(bf16[16,16,128]{2,0,1:T(8,128)(2,1)} %copy_bitcast_fusion.1), calls=%async_computation | async-start | bytes 131072 | tf_op jit(solution)/shard_map/all_to_all | solution.py:133
  18.2 1.9 collective-permute-start
  20.1 1.3 collective-permute-start.1
  21.6 1.7 copy_bitcast_fusion
  24.1 1.9 collective-permute-done.1
  26.5 1.3 fusion.51
  27.8 7.2 %all-to-all-start.2 = ((bf16[64,16,128]{2,0,1:T(8,128)(2,1)}), bf16[64,16,128]{2,0,1:T(8,128)(2,1)S(1)}, u32[]{:S(2)}, u32[]{:S(2)}) async-start(bf16[64,16,128]{2,0,1:T(8,128)(2,1)} %copy_bitcast_fusion), calls=%async_computation.2 | async-start | bytes 524288 | tf_op jit(solution)/shard_map/all_to_all | solution.py:132
  35.4 9.2 %all-to-all-done.2 = bf16[64,16,128]{2,0,1:T(8,128)(2,1)S(1)} async-done(((bf16[64,16,128]{2,0,1:T(8,128)(2,1)}), bf16[64,16,128]{2,0,1:T(8,128)(2,1)S(1)}, u32[]{:S(2)}, u32[]{:S(2)}) %all-to-all-start.2) | async-done | bytes 262176 | tf_op jit(solution)/shard_map/all_to_all | solution.py:132
  45.5 5.0 %all-to-all-start.1 = ((bf16[16,256,64]{1,2,0:T(8,128)(2,1)}), bf16[16,256,64]{1,2,0:T(8,128)(2,1)S(1)}, u32[]{:S(2)}, u32[]{:S(2)}) async-start(bf16[16,256,64]{1,2,0:T(8,128)(2,1)} %broadcast_in_dim.11), calls=%async_computation.1 | async-start | bytes 1048576 | tf_op jit(solution)/shard_map/all_to_all | solution.py:37
  50.7 14.4 %all-to-all-done.1 = bf16[16,256,64]{1,2,0:T(8,128)(2,1)S(1)} async-done(((bf16[16,256,64]{1,2,0:T(8,128)(2,1)}), bf16[16,256,64]{1,2,0:T(8,128)(2,1)S(1)}, u32[]{:S(2)}, u32[]{:S(2)}) %all-to-all-start.1) | async-done | bytes 524320 | tf_op jit(solution)/shard_map/all_to_all | solution.py:37
  66.0 5.7 %all-to-all-start.3 = ((f32[16,1,256]{2,1,0:T(1,128)}), f32[16,1,256]{2,1,0:T(1,128)S(1)}, u32[]{:S(2)}, u32[]{:S(2)}) async-start(f32[16,1,256]{2,1,0:T(1,128)} %broadcast_in_dim.12), calls=%async_computation.3 | async-start | bytes 32768 | tf_op jit(solution)/shard_map/all_to_all | solution.py:37
  72.4 5.5 %all-to-all-done.3 = f32[16,1,256]{2,1,0:T(1,128)S(1)} async-done(((f32[16,1,256]{2,1,0:T(1,128)}), f32[16,1,256]{2,1,0:T(1,128)S(1)}, u32[]{:S(2)}, u32[]{:S(2)}) %all-to-all-start.3) | async-done | bytes 16416 | tf_op jit(solution)/shard_map/all_to_all | solution.py:37
  78.1 1.1 broadcast_in_dim.13
  79.2 4.9 %all-to-all-start.4 = ((bf16[16,256,128]{1,2,0:T(8,128)(2,1)}), bf16[16,256,128]{1,2,0:T(8,128)(2,1)S(1)}, u32[]{:S(2)}, u32[]{:S(2)}) async-start(bf16[16,256,128]{1,2,0:T(8,128)(2,1)} %broadcast_in_dim.13), calls=%async_computation.4 | async-start | bytes 2097152 | tf_op jit(solution)/shard_map/all_to_all | solution.py:37
  84.7 1.4 select_reduce_fusion.1
  87.2 21.5 %all-to-all-done.4 = bf16[16,256,128]{1,2,0:T(8,128)(2,1)S(1)} async-done(((bf16[16,256,128]{1,2,0:T(8,128)(2,1)}), bf16[16,256,128]{1,2,0:T(8,128)(2,1)S(1)}, u32[]{:S(2)}, u32[]{:S(2)}) %all-to-all-start.4) | async-done | bytes 1048608 | tf_op jit(solution)/shard_map/all_to_all | solution.py:37
  109.8 1.3 reshape_reshape.2
  111.1 1.2 convolution_convert_fusion
  112.4 33.3 %all_to_all.59 = bf16[32,4,2048]{2,1,0:T(4,128)(2,1)S(1)} all-to-all(bf16[32,4,2048]{2,1,0:T(4,128)(2,1)S(1)} %all_to_all.49), channel_id=1, replica_groups=mesh['sp'=32,'tp'=16] {'sp'}, dimensions={0} | all-to-all | bytes 1048576 | tf_op jit(solution)/shard_map/all_to_all | solution.py:156
  145.7 1.1 copy.142
  147.4 1.2 fusion.18
  148.8 50.0 %all-gather.3.cloned.1.call-done = bf16[16,32,2,2,2048]{4,1,3,0,2:T(8,128)(2,1)} async-done(((bf16[1,32,2,2,2048]{4,1,3,0,2:T(8,128)(2,1)}), bf16[16,32,2,2,2048]{4,1,3,0,2:T(8,128)(2,1)}) %all-gather.3.cloned.1.call-update) | async-done | bytes 8388624 | tf_op jit(solution)/shard_map/all_gather | solution.py:158
  198.8 5.8 %convolution_bitcast_fusion.1 = f32[64,16,32,2,2]{0,2,4,1,3:T(8,128)S(1)} fusion(bf16[16,32,2,2,2048]{4,1,3,0,2:T(8,128)(2,1)} %all-gather.3.cloned.1.call-done, bf16[2,64,2048]{2,1,0:T(8,128)(2,1)S(1)} %copy-done.2), kind=kOutput, calls=%fused_computation.6 | convolution fusion | flops 536870912 | bytes 9437184 | tf_op jit(solution)/shard_map/tsecd,efd->tsecf/dot_general | solution.py:159
  204.7 2.3 fusion.4
  208.6 44.9 %all-gather.5.cloned.1.call-done = bf16[1024,2304]{1,0:T(8,128)(2,1)} async-done(((bf16[64,2304]{1,0:T(8,128)(2,1)}), bf16[1024,2304]{1,0:T(8,128)(2,1)}) %all-gather.5.cloned.1.call-update) | async-done | bytes 4718608 | tf_op jit(solution)/shard_map/all_gather | solution.py:52
  253.5 4.8 %split.8 = bf16[1024,2048]{1,0:T(8,128)(2,1)} slice(bf16[1024,2304]{1,0:T(8,128)(2,1)} %all-gather.5.cloned.1.call-done), slice={[0:1024], [0:2048]} | slice | bytes 8388608 | tf_op jit(solution)/shard_map/split | solution.py:53
  258.3 6.5 %copy.146 = bf16[1024,2048]{0,1:T(8,128)(2,1)} copy(bf16[1024,2048]{1,0:T(8,128)(2,1)} %split.8) | data formatting | bytes 8388608 | tf_op jit(solution)/shard_map/split | solution.py:53
  264.8 7.2 %reshape.237 = bf16[1024,16,32,2,2]{0,4,3,2,1:T(2,128)(2,1)} reshape(bf16[1024,2048]{0,1:T(8,128)(2,1)} %copy.146) | data formatting | bytes 8388608 | tf_op jit(solution)/shard_map/reshape | solution.py:56
  272.0 3.6 %fusion.8 = bf16[16,32,2,2,128]{4,1,3,0,2:T(8,128)(2,1)S(1)} fusion(bf16[1024,16,32,2,2]{0,4,3,2,1:T(2,128)(2,1)} %reshape.237, bf16[2,1024,128]{2,1,0:T(8,128)(2,1)S(1)} %copy-done), kind=kOutput, calls=%fused_computation.9 | convolution fusion | flops 537133056 | bytes 5242880 | tf_op jit(solution)/shard_map/tsecf,efd->tsecd/dot_general | solution.py:172
  276.2 28.2 %all_to_all.60 = bf16[16,32,2,2,128]{4,3,0,2,1:T(2,128)(2,1)S(1)} all-to-all(bf16[16,32,2,2,128]{4,3,0,2,1:T(2,128)(2,1)S(1)} %copy.148), channel_id=1, replica_groups=mesh['sp'=32,'tp'=16] {'sp'}, dimensions={1} | all-to-all | bytes 1048576 | tf_op jit(solution)/shard_map/all_to_all | solution.py:178
  304.9 1.3 fusion.16
  (74 shorter events, 11.8 us)
Async XLA Ops:
  6.5 265.5 %copy-start = (bf16[2,1024,128]{2,1,0:T(8,128)(2,1)S(1)}, bf16[2,1024,128]{2,1,0:T(8,128)(2,1)}, u32[]{:S(2)}) copy-start(bf16[2,1024,128]{2,1,0:T(8,128)(2,1)} %param.26) | copy-start | bytes 1572868
  8.1 19.8 %all-to-all-start = ((bf16[16,16,128]{2,0,1:T(8,128)(2,1)}), bf16[16,16,128]{2,0,1:T(8,128)(2,1)S(1)}, u32[]{:S(2)}, u32[]{:S(2)}) async-start(bf16[16,16,128]{2,0,1:T(8,128)(2,1)} %copy_bitcast_fusion.1), calls=%async_computation | async-start | bytes 131072 | tf_op jit(solution)/shard_map/all_to_all | solution.py:133
  18.2 5.8 %collective-permute-start = (bf16[128,128]{1,0:T(8,128)(2,1)S(1)}, bf16[128,128]{1,0:T(8,128)(2,1)S(1)}, u32[]{:S(2)}, u32[]{:S(2)}) collective-permute-start(bf16[128,128]{1,0:T(8,128)(2,1)S(1)} %get-tuple-element.10), channel_id=1, source_target_pairs={{0,16},{16,32},{32,48},{48,64},{64,80},{80,96},{96,112},{112,128},... | collective-permute-start | bytes 98312 | tf_op jit(solution)/shard_map/ppermute | solution.py:23
  20.1 5.8 %collective-permute-start.1 = (bf16[128,128]{1,0:T(8,128)(2,1)S(1)}, bf16[128,128]{1,0:T(8,128)(2,1)S(1)}, u32[]{:S(2)}, u32[]{:S(2)}) collective-permute-start(bf16[128,128]{1,0:T(8,128)(2,1)S(1)} %get-tuple-element.11), channel_id=1, source_target_pairs={{16,0},{32,16},{48,32},{64,48},{80,64},{96,80},{112,96},{128,112},... | collective-permute-start | bytes 98312 | tf_op jit(solution)/shard_map/ppermute | solution.py:24
  27.8 56.3 %copy-start.6 = (s32[256,4]{0,1:T(4,128)S(1)}, s32[256,4]{0,1:T(4,128)}, u32[]{:S(2)}) copy-start(s32[256,4]{0,1:T(4,128)} %param.22) | copy-start | bytes 12292
  27.8 56.5 %copy-start.7 = (f32[256,4]{0,1:T(4,128)S(1)}, f32[256,4]{0,1:T(4,128)}, u32[]{:S(2)}) copy-start(f32[256,4]{0,1:T(4,128)} %param.23) | copy-start | bytes 12292
  27.8 16.8 %all-to-all-start.2 = ((bf16[64,16,128]{2,0,1:T(8,128)(2,1)}), bf16[64,16,128]{2,0,1:T(8,128)(2,1)S(1)}, u32[]{:S(2)}, u32[]{:S(2)}) async-start(bf16[64,16,128]{2,0,1:T(8,128)(2,1)} %copy_bitcast_fusion), calls=%async_computation.2 | async-start | bytes 524288 | tf_op jit(solution)/shard_map/all_to_all | solution.py:132
  45.5 19.5 %all-to-all-start.1 = ((bf16[16,256,64]{1,2,0:T(8,128)(2,1)}), bf16[16,256,64]{1,2,0:T(8,128)(2,1)S(1)}, u32[]{:S(2)}, u32[]{:S(2)}) async-start(bf16[16,256,64]{1,2,0:T(8,128)(2,1)} %broadcast_in_dim.11), calls=%async_computation.1 | async-start | bytes 1048576 | tf_op jit(solution)/shard_map/all_to_all | solution.py:37
  66.0 12.0 %all-to-all-start.3 = ((f32[16,1,256]{2,1,0:T(1,128)}), f32[16,1,256]{2,1,0:T(1,128)S(1)}, u32[]{:S(2)}, u32[]{:S(2)}) async-start(f32[16,1,256]{2,1,0:T(1,128)} %broadcast_in_dim.12), calls=%async_computation.3 | async-start | bytes 32768 | tf_op jit(solution)/shard_map/all_to_all | solution.py:37
  79.2 29.6 %all-to-all-start.4 = ((bf16[16,256,128]{1,2,0:T(8,128)(2,1)}), bf16[16,256,128]{1,2,0:T(8,128)(2,1)S(1)}, u32[]{:S(2)}, u32[]{:S(2)}) async-start(bf16[16,256,128]{1,2,0:T(8,128)(2,1)} %broadcast_in_dim.13), calls=%async_computation.4 | async-start | bytes 2097152 | tf_op jit(solution)/shard_map/all_to_all | solution.py:37
  84.1 114.7 %all-gather.3.cloned.1.call-start = ((), (), s32[]{:S(2)}) async-start(), calls=%async_computation.7 | async-start | bytes 8912896 | tf_op jit(solution)/shard_map/all_gather | solution.py:158
  84.1 63.0 %copy-start.4 = (bf16[64,2048]{1,0:T(8,128)(2,1)S(1)}, bf16[64,2048]{1,0:T(8,128)(2,1)}, u32[]{:S(2)}) copy-start(bf16[64,2048]{1,0:T(8,128)(2,1)} %param.27) | copy-start | bytes 786436
  109.8 89.0 %copy-start.2 = (bf16[2,64,2048]{2,1,0:T(8,128)(2,1)S(1)}, bf16[2,64,2048]{2,1,0:T(8,128)(2,1)}, u32[]{:S(2)}) copy-start(bf16[2,64,2048]{2,1,0:T(8,128)(2,1)} %param.24) | copy-start | bytes 1572868
  146.8 106.7 %all-gather.5.cloned.1.call-start = ((), (), s32[]{:S(2)}) async-start(), calls=%async_computation.8 | async-start | bytes 5013504 | tf_op jit(solution)/shard_map/all_gather | solution.py:52
  148.8 55.9 %copy-start.8 = (bf16[2,64,2048]{2,1,0:T(8,128)(2,1)S(1)}, bf16[2,64,2048]{2,1,0:T(8,128)(2,1)}, u32[]{:S(2)}) copy-start(bf16[2,64,2048]{2,1,0:T(8,128)(2,1)} %param.25) | copy-start | bytes 1572868
  198.8 5.9 %copy-start.1 = (bf16[16,32,2,2,2048]{4,1,3,0,2:T(8,128)(2,1)S(1)}, bf16[16,32,2,2,2048]{4,1,3,0,2:T(8,128)(2,1)}, u32[]{:S(2)}) copy-start(bf16[16,32,2,2,2048]{4,1,3,0,2:T(8,128)(2,1)} %all-gather.3.cloned.1.call-done) | copy-start | bytes 25165828
  272.0 32.5 %copy-start.5 = (bf16[16,128,16]{1,2,0:T(8,128)(2,1)S(1)}, bf16[16,128,16]{1,2,0:T(8,128)(2,1)}, u32[]{:S(2)}) copy-start(bf16[16,128,16]{1,2,0:T(8,128)(2,1)} %get-tuple-element.5) | copy-start | bytes 196612
  272.0 32.8 %copy-start.3 = (bf16[1024,128]{1,0:T(8,128)(2,1)S(1)}, bf16[1024,128]{1,0:T(8,128)(2,1)}, u32[]{:S(2)}) copy-start(bf16[1024,128]{1,0:T(8,128)(2,1)} %param.29) | copy-start | bytes 786436
Sparse Core Ops, SparseCore 0:
  147.0 51.7 all-gather.2
  208.7 44.7 all-gather.4
where the time goes:
time: 315 us; the launch traced here: 314 us
  waiting for transfers between devices  147 us (47%)
  blocking collectives  61.5 us (20%)
  starting transfers between devices  35.4 us (11%)
  local copies, waits for them, and re-layouts  33.1 us (11%)
  matrix products  17.8 us (6%)
  between operations  14.5 us (5%)
  other arithmetic  4.01 us (1%)
    all_gather x1, waiting for transfers between devices, local(): piece_rows = lax.all_gather(arrived, 'tp', axis=0, tiled=True)  50 us
    all_gather x1, waiting for transfers between devices, gather_turned(): result = lax.all_gather(both, axis, axis=0, tiled=True)  44.9 us
    all_to_all x3, waiting for transfers between devices, from_everyone(): return lax.all_to_all(copies, axis, split_axis=0, concat_axis=0, tiled=True)  41.4 us
    all_to_all x1, blocking collectives, local(): lax.all_to_all(outgoing, 'sp', split_axis=0, concat_axis=0, tiled=True)  33.3 us
    all_to_all x1, blocking collectives, local(): lax.all_to_all(routed_total.astype(jnp.bfloat16), 'sp', split_axis=1, con...  28.2 us
    all_to_all x3, starting transfers between devices, from_everyone(): return lax.all_to_all(copies, axis, split_axis=0, concat_axis=0, tiled=True)  15.6 us
    split x2, local copies, waits for them, and re-layouts, gather_turned(): jnp.split(result, [sum(widths[:k]) for k in range(1, len(widths))], axis=1)  11.3 us
    all_to_all x1, waiting for transfers between devices, local(): lax.all_to_all(w_out, 'tp', split_axis=1, concat_axis=0, tiled=True)  9.24 us
  transfers between devices with their start and end apart: 9, of which 7 were waited for; matrix products, arithmetic and copies ran while one was open for 3% of the time, Pallas kernels for 0%

commit v1 on v0

--- a/solution.py
+++ b/solution.py
@@ -155,7 +155,9 @@
     outgoing = jnp.dot(own_table, own_rows, preferred_element_type=jnp.float32).astype(jnp.bfloat16)
     arrived = lax.all_to_all(outgoing, "sp", split_axis=0, concat_axis=0, tiled=True)
     arrived = arrived.reshape(1, n_sp, exp_dev, capacity, D)
-    piece_rows = lax.all_gather(arrived, "tp", axis=0, tiled=True)
+    piece_rows = jnp.concatenate(
+        lax.all_to_all(jnp.stack([arrived] * lax.axis_size("tp")), "tp", 0, 0), axis=0
+    )
     gate_act = jnp.einsum(
         "tsecd,efd->tsecf", piece_rows, w_gate, preferred_element_type=jnp.float32
     )

time: 315 us -> 454 us (1.44)
  waiting for transfers between devices: 147 us -> 275 us
  starting transfers between devices: 35.4 us -> 42.1 us
    all_to_all x0 -> x1, waiting for transfers between devices: none -> 181 us  [local(): lax.all_to_all(jnp.stack([arrived] * lax.axis_size('tp')), 'tp', 0, 0)]
    all_gather x1 -> x0, waiting for transfers between devices: 50 us -> none  [local(): piece_rows = lax.all_gather(arrived, 'tp', axis=0, tiled=True)]
    all_to_all x0 -> x1, starting transfers between devices: none -> 6.74 us  [local(): lax.all_to_all(jnp.stack([arrived] * lax.axis_size('tp')), 'tp', 0, 0)]
    all_gather x1, waiting for transfers between devices: 44.9 us -> 40 us  [gather_turned(): result = lax.all_gather(both, axis, axis=0, tiled=True)]
    another operation x0 -> x2, local copies, waits for them, and re-layouts: none -> 4.6 us  [local(): jnp.stack([arrived] * lax.axis_size('tp'))]
  transfers between devices with their start and end apart: 9 -> 9, of which waited for: 7 -> 7; matrix products, arithmetic and copies ran while one was open for 3% -> 2% of each run, Pallas kernels for 0% -> 0%
where the time goes in v1:
time: 454 us; the launch traced here: 453 us
  waiting for transfers between devices  275 us (61%)
  blocking collectives  61.5 us (14%)
  starting transfers between devices  42.1 us (9%)
  local copies, waits for them, and re-layouts  36.6 us (8%)
  matrix products  20.1 us (4%)
  between operations  14.4 us (3%)
    all_to_all x1, waiting for transfers between devices, local(): lax.all_to_all(jnp.stack([arrived] * lax.axis_size('tp')), 'tp', 0, 0)  181 us
    all_to_all x3, waiting for transfers between devices, from_everyone(): return lax.all_to_all(copies, axis, split_axis=0, concat_axis=0, tiled=True)  42.1 us
    all_gather x1, waiting for transfers between devices, gather_turned(): result = lax.all_gather(both, axis, axis=0, tiled=True)  40 us
    all_to_all x1, blocking collectives, local(): lax.all_to_all(outgoing, 'sp', split_axis=0, concat_axis=0, tiled=True)  33.2 us
    all_to_all x1, blocking collectives, local(): lax.all_to_all(routed_total.astype(jnp.bfloat16), 'sp', split_axis=1, con...  28.2 us
    all_to_all x3, starting transfers between devices, from_everyone(): return lax.all_to_all(copies, axis, split_axis=0, concat_axis=0, tiled=True)  15.6 us
    split x2, local copies, waits for them, and re-layouts, gather_turned(): jnp.split(result, [sum(widths[:k]) for k in range(1, len(widths))], axis=1)  11.3 us
    all_to_all x1, waiting for transfers between devices, local(): lax.all_to_all(w_out, 'tp', split_axis=1, concat_axis=0, tiled=True)  9.24 us
  transfers between devices with their start and end apart: 9, of which 7 were waited for; matrix products, arithmetic and copies ran while one was open for 2% of the time, Pallas kernels for 0%

profile of v1, /device:TPU:8, one launch (start us, length us, event | category | flops | bytes accessed | tf_op | source)
XLA Modules:
  0.0 452.5 jit_solution(2030757616792752890)
XLA Ops:
  6.5 1.5 copy_bitcast_fusion.1
  8.1 9.1 %all-to-all-start = ((bf16[16,16,128]{2,0,1:T(8,128)(2,1)}), bf16[16,16,128]{2,0,1:T(8,128)(2,1)S(1)}, u32[]{:S(2)}, u32[]{:S(2)}) async-start(bf16[16,16,128]{2,0,1:T(8,128)(2,1)} %copy_bitcast_fusion.1), calls=%async_computation | async-start | bytes 131072 | tf_op jit(solution)/shard_map/all_to_all | solution.py:133
  18.2 1.9 collective-permute-start
  20.1 1.3 collective-permute-start.1
  21.6 1.7 copy_bitcast_fusion
  24.0 1.9 collective-permute-done.1
  26.5 1.3 fusion.67
  27.8 7.2 %all-to-all-start.2 = ((bf16[64,16,128]{2,0,1:T(8,128)(2,1)}), bf16[64,16,128]{2,0,1:T(8,128)(2,1)S(1)}, u32[]{:S(2)}, u32[]{:S(2)}) async-start(bf16[64,16,128]{2,0,1:T(8,128)(2,1)} %copy_bitcast_fusion), calls=%async_computation.2 | async-start | bytes 524288 | tf_op jit(solution)/shard_map/all_to_all | solution.py:132
  35.4 9.2 %all-to-all-done.2 = bf16[64,16,128]{2,0,1:T(8,128)(2,1)S(1)} async-done(((bf16[64,16,128]{2,0,1:T(8,128)(2,1)}), bf16[64,16,128]{2,0,1:T(8,128)(2,1)S(1)}, u32[]{:S(2)}, u32[]{:S(2)}) %all-to-all-start.2) | async-done | bytes 262176 | tf_op jit(solution)/shard_map/all_to_all | solution.py:132
  45.5 5.0 %all-to-all-start.1 = ((bf16[16,256,64]{1,2,0:T(8,128)(2,1)}), bf16[16,256,64]{1,2,0:T(8,128)(2,1)S(1)}, u32[]{:S(2)}, u32[]{:S(2)}) async-start(bf16[16,256,64]{1,2,0:T(8,128)(2,1)} %broadcast_in_dim.11), calls=%async_computation.1 | async-start | bytes 1048576 | tf_op jit(solution)/shard_map/all_to_all | solution.py:37
  50.7 14.4 %all-to-all-done.1 = bf16[16,256,64]{1,2,0:T(8,128)(2,1)S(1)} async-done(((bf16[16,256,64]{1,2,0:T(8,128)(2,1)}), bf16[16,256,64]{1,2,0:T(8,128)(2,1)S(1)}, u32[]{:S(2)}, u32[]{:S(2)}) %all-to-all-start.1) | async-done | bytes 524320 | tf_op jit(solution)/shard_map/all_to_all | solution.py:37
  66.0 5.7 %all-to-all-start.3 = ((f32[16,1,256]{2,1,0:T(1,128)}), f32[16,1,256]{2,1,0:T(1,128)S(1)}, u32[]{:S(2)}, u32[]{:S(2)}) async-start(f32[16,1,256]{2,1,0:T(1,128)} %broadcast_in_dim.12), calls=%async_computation.3 | async-start | bytes 32768 | tf_op jit(solution)/shard_map/all_to_all | solution.py:37
  72.4 5.5 %all-to-all-done.3 = f32[16,1,256]{2,1,0:T(1,128)S(1)} async-done(((f32[16,1,256]{2,1,0:T(1,128)}), f32[16,1,256]{2,1,0:T(1,128)S(1)}, u32[]{:S(2)}, u32[]{:S(2)}) %all-to-all-start.3) | async-done | bytes 16416 | tf_op jit(solution)/shard_map/all_to_all | solution.py:37
  79.2 4.9 %all-to-all-start.4 = ((bf16[16,256,128]{1,2,0:T(8,128)(2,1)}), bf16[16,256,128]{1,2,0:T(8,128)(2,1)S(1)}, u32[]{:S(2)}, u32[]{:S(2)}) async-start(bf16[16,256,128]{1,2,0:T(8,128)(2,1)} %broadcast_in_dim.13), calls=%async_computation.4 | async-start | bytes 2097152 | tf_op jit(solution)/shard_map/all_to_all | solution.py:37
  84.6 1.4 select_reduce_fusion.1
  86.5 22.2 %all-to-all-done.4 = bf16[16,256,128]{1,2,0:T(8,128)(2,1)S(1)} async-done(((bf16[16,256,128]{1,2,0:T(8,128)(2,1)}), bf16[16,256,128]{1,2,0:T(8,128)(2,1)S(1)}, u32[]{:S(2)}, u32[]{:S(2)}) %all-to-all-start.4) | async-done | bytes 1048608 | tf_op jit(solution)/shard_map/all_to_all | solution.py:37
  108.7 1.1 copy.143
  109.8 1.3 reshape_reshape.2
  111.1 1.2 convolution_convert_fusion
  112.4 33.2 %all_to_all.64 = bf16[32,4,2048]{2,1,0:T(4,128)(2,1)S(1)} all-to-all(bf16[32,4,2048]{2,1,0:T(4,128)(2,1)S(1)} %all_to_all.52), channel_id=1, replica_groups=mesh['sp'=32,'tp'=16] {'sp'}, dimensions={0} | all-to-all | bytes 1048576 | tf_op jit(solution)/shard_map/all_to_all | solution.py:156
  146.0 4.3 stack.3
  150.3 6.7 %all-to-all-start.6 = ((bf16[16,1,32,2,2,2048]{5,2,4,3,1,0:T(8,128)(2,1)}), bf16[16,1,32,2,2,2048]{5,2,4,3,1,0:T(8,128)(2,1)}, u32[]{:S(2)}, u32[]{:S(2)}) async-start(bf16[16,1,32,2,2,2048]{5,2,4,3,1,0:T(8,128)(2,1)} %stack.3), calls=%async_computation.6 | async-start | bytes 16777216 | tf_op jit(solution)/shard_map/all_to_all | solution.py:159
  158.0 181.3 %all-to-all-done.6 = bf16[16,1,32,2,2,2048]{5,2,4,3,1,0:T(8,128)(2,1)} async-done(((bf16[16,1,32,2,2,2048]{5,2,4,3,1,0:T(8,128)(2,1)}), bf16[16,1,32,2,2,2048]{5,2,4,3,1,0:T(8,128)(2,1)}, u32[]{:S(2)}, u32[]{:S(2)}) %all-to-all-start.6) | async-done | bytes 8388640 | tf_op jit(solution)/shard_map/all_to_all | solution.py:159
  339.3 5.7 %fusion.9 = f32[64,16,32,2,2]{0,2,4,1,3:T(8,128)S(1)} fusion(bf16[16,1,32,2,2,2048]{5,2,4,3,1,0:T(8,128)(2,1)} %all-to-all-done.6, bf16[2,64,2048]{2,1,0:T(8,128)(2,1)S(1)} %copy-done.6), kind=kOutput, calls=%fused_computation.10 | convolution fusion | flops 536870912 | bytes 9437184 | tf_op jit(solution)/shard_map/tsecd,efd->tsecf/dot_general | solution.py:161
  345.0 5.7 %fusion.18 = bf16[64,16,32,2,2]{0,2,4,1,3:T(8,128)(2,1)S(1)} fusion(bf16[16,1,32,2,2,2048]{5,2,4,3,1,0:T(8,128)(2,1)} %all-to-all-done.6, f32[64,16,32,2,2]{0,2,4,1,3:T(8,128)S(1)} %fusion.9, bf16[2,64,2048]{2,1,0:T(8,128)(2,1)S(1)} %copy-done.7), kind=kOutput, calls=%fused_computation.13 | convolution fusion | flops 537657344 | bytes 9699328 | tf_op jit(solution)/shard_map/tsecd,efd->tsecf/dot_general | solution.py:164
  352.3 40.0 %all-gather.2.cloned.1.call-done = bf16[1024,2304]{1,0:T(8,128)(2,1)} async-done(((bf16[64,2304]{1,0:T(8,128)(2,1)}), bf16[1024,2304]{1,0:T(8,128)(2,1)}) %all-gather.2.cloned.1.call-update) | async-done | bytes 4718608 | tf_op jit(solution)/shard_map/all_gather | solution.py:52
  392.3 4.8 %split.8 = bf16[1024,2048]{1,0:T(8,128)(2,1)} slice(bf16[1024,2304]{1,0:T(8,128)(2,1)} %all-gather.2.cloned.1.call-done), slice={[0:1024], [0:2048]} | slice | bytes 8388608 | tf_op jit(solution)/shard_map/split | solution.py:53
  397.1 6.5 %copy.149 = bf16[1024,2048]{0,1:T(8,128)(2,1)} copy(bf16[1024,2048]{1,0:T(8,128)(2,1)} %split.8) | data formatting | bytes 8388608 | tf_op jit(solution)/shard_map/split | solution.py:53
  403.6 7.2 %reshape.241 = bf16[1024,16,32,2,2]{0,4,3,2,1:T(2,128)(2,1)} reshape(bf16[1024,2048]{0,1:T(8,128)(2,1)} %copy.149) | data formatting | bytes 8388608 | tf_op jit(solution)/shard_map/reshape | solution.py:56
  410.8 3.6 fusion.24
  414.9 28.2 %all_to_all.65 = bf16[16,32,2,2,128]{4,3,0,2,1:T(2,128)(2,1)S(1)} all-to-all(bf16[16,32,2,2,128]{4,3,0,2,1:T(2,128)(2,1)S(1)} %copy.151), channel_id=1, replica_groups=mesh['sp'=32,'tp'=16] {'sp'}, dimensions={1} | all-to-all | bytes 1048576 | tf_op jit(solution)/shard_map/all_to_all | solution.py:180
  443.6 1.3 fusion.32
  (72 shorter events, 11.7 us)
Async XLA Ops:
  6.5 404.3 %copy-start = (bf16[2,1024,128]{2,1,0:T(8,128)(2,1)S(1)}, bf16[2,1024,128]{2,1,0:T(8,128)(2,1)}, u32[]{:S(2)}) copy-start(bf16[2,1024,128]{2,1,0:T(8,128)(2,1)} %param.26) | copy-start | bytes 1572868
  8.1 19.8 %all-to-all-start = ((bf16[16,16,128]{2,0,1:T(8,128)(2,1)}), bf16[16,16,128]{2,0,1:T(8,128)(2,1)S(1)}, u32[]{:S(2)}, u32[]{:S(2)}) async-start(bf16[16,16,128]{2,0,1:T(8,128)(2,1)} %copy_bitcast_fusion.1), calls=%async_computation | async-start | bytes 131072 | tf_op jit(solution)/shard_map/all_to_all | solution.py:133
  18.2 5.8 %collective-permute-start = (bf16[128,128]{1,0:T(8,128)(2,1)S(1)}, bf16[128,128]{1,0:T(8,128)(2,1)S(1)}, u32[]{:S(2)}, u32[]{:S(2)}) collective-permute-start(bf16[128,128]{1,0:T(8,128)(2,1)S(1)} %get-tuple-element.10), channel_id=1, source_target_pairs={{0,16},{16,32},{32,48},{48,64},{64,80},{80,96},{96,112},{112,128},... | collective-permute-start | bytes 98312 | tf_op jit(solution)/shard_map/ppermute | solution.py:23
  20.1 5.8 %collective-permute-start.1 = (bf16[128,128]{1,0:T(8,128)(2,1)S(1)}, bf16[128,128]{1,0:T(8,128)(2,1)S(1)}, u32[]{:S(2)}, u32[]{:S(2)}) collective-permute-start(bf16[128,128]{1,0:T(8,128)(2,1)S(1)} %get-tuple-element.11), channel_id=1, source_target_pairs={{16,0},{32,16},{48,32},{64,48},{80,64},{96,80},{112,96},{128,112},... | collective-permute-start | bytes 98312 | tf_op jit(solution)/shard_map/ppermute | solution.py:24
  27.8 56.3 %copy-start.4 = (s32[256,4]{0,1:T(4,128)S(1)}, s32[256,4]{0,1:T(4,128)}, u32[]{:S(2)}) copy-start(s32[256,4]{0,1:T(4,128)} %param.22) | copy-start | bytes 12292
  27.8 56.5 %copy-start.5 = (f32[256,4]{0,1:T(4,128)S(1)}, f32[256,4]{0,1:T(4,128)}, u32[]{:S(2)}) copy-start(f32[256,4]{0,1:T(4,128)} %param.23) | copy-start | bytes 12292
  27.8 16.8 %all-to-all-start.2 = ((bf16[64,16,128]{2,0,1:T(8,128)(2,1)}), bf16[64,16,128]{2,0,1:T(8,128)(2,1)S(1)}, u32[]{:S(2)}, u32[]{:S(2)}) async-start(bf16[64,16,128]{2,0,1:T(8,128)(2,1)} %copy_bitcast_fusion), calls=%async_computation.2 | async-start | bytes 524288 | tf_op jit(solution)/shard_map/all_to_all | solution.py:132
  45.5 19.5 %all-to-all-start.1 = ((bf16[16,256,64]{1,2,0:T(8,128)(2,1)}), bf16[16,256,64]{1,2,0:T(8,128)(2,1)S(1)}, u32[]{:S(2)}, u32[]{:S(2)}) async-start(bf16[16,256,64]{1,2,0:T(8,128)(2,1)} %broadcast_in_dim.11), calls=%async_computation.1 | async-start | bytes 1048576 | tf_op jit(solution)/shard_map/all_to_all | solution.py:37
  66.0 12.0 %all-to-all-start.3 = ((f32[16,1,256]{2,1,0:T(1,128)}), f32[16,1,256]{2,1,0:T(1,128)S(1)}, u32[]{:S(2)}, u32[]{:S(2)}) async-start(f32[16,1,256]{2,1,0:T(1,128)} %broadcast_in_dim.12), calls=%async_computation.3 | async-start | bytes 32768 | tf_op jit(solution)/shard_map/all_to_all | solution.py:37
  79.2 29.6 %all-to-all-start.4 = ((bf16[16,256,128]{1,2,0:T(8,128)(2,1)}), bf16[16,256,128]{1,2,0:T(8,128)(2,1)S(1)}, u32[]{:S(2)}, u32[]{:S(2)}) async-start(bf16[16,256,128]{1,2,0:T(8,128)(2,1)} %broadcast_in_dim.13), calls=%async_computation.4 | async-start | bytes 2097152 | tf_op jit(solution)/shard_map/all_to_all | solution.py:37
  150.3 7.0 %copy-start.2 = (bf16[64,2048]{1,0:T(8,128)(2,1)S(1)}, bf16[64,2048]{1,0:T(8,128)(2,1)}, u32[]{:S(2)}) copy-start(bf16[64,2048]{1,0:T(8,128)(2,1)} %param.27) | copy-start | bytes 786436
  150.3 7.3 %copy-start.3 = (bf16[64,2048]{1,0:T(8,128)(2,1)S(1)}, bf16[64,2048]{1,0:T(8,128)(2,1)}, u32[]{:S(2)}) copy-start(bf16[64,2048]{1,0:T(8,128)(2,1)} %param.28) | copy-start | bytes 786436
  150.3 189.0 %copy-start.6 = (bf16[2,64,2048]{2,1,0:T(8,128)(2,1)S(1)}, bf16[2,64,2048]{2,1,0:T(8,128)(2,1)}, u32[]{:S(2)}) copy-start(bf16[2,64,2048]{2,1,0:T(8,128)(2,1)} %param.24) | copy-start | bytes 1572868
  150.3 189.0 %all-to-all-start.6 = ((bf16[16,1,32,2,2,2048]{5,2,4,3,1,0:T(8,128)(2,1)}), bf16[16,1,32,2,2,2048]{5,2,4,3,1,0:T(8,128)(2,1)}, u32[]{:S(2)}, u32[]{:S(2)}) async-start(bf16[16,1,32,2,2,2048]{5,2,4,3,1,0:T(8,128)(2,1)} %stack.3), calls=%async_computation.6 | async-start | bytes 16777216 | tf_op jit(solution)/shard_map/all_to_all | solution.py:159
  157.0 235.3 %all-gather.2.cloned.1.call-start = ((), (), s32[]{:S(2)}) async-start(), calls=%async_computation.8 | async-start | bytes 5013504 | tf_op jit(solution)/shard_map/all_gather | solution.py:52
  158.0 187.0 %copy-start.7 = (bf16[2,64,2048]{2,1,0:T(8,128)(2,1)S(1)}, bf16[2,64,2048]{2,1,0:T(8,128)(2,1)}, u32[]{:S(2)}) copy-start(bf16[2,64,2048]{2,1,0:T(8,128)(2,1)} %param.25) | copy-start | bytes 1572868
  410.8 32.8 %copy-start.1 = (bf16[1024,128]{1,0:T(8,128)(2,1)S(1)}, bf16[1024,128]{1,0:T(8,128)(2,1)}, u32[]{:S(2)}) copy-start(bf16[1024,128]{1,0:T(8,128)(2,1)} %param.29) | copy-start | bytes 786436
Sparse Core Ops, SparseCore 0:
  352.4 39.8 all-gather.1
